TPU v7x, 32 devices: a whole 2x2x4 slice. The times are simulated.
32 devices in a mesh: fs: 8 (over z, y), tp: 4 (over x, core).
Axes of the slice: x: 2, y: 2, z: 4, core: 2. Of those that a mesh axis runs over, the one named last changes fastest.
Arguments:
- prompt_tokens: bfloat16 [4, 128, 4096], P('tp'), may hold values from -6 to 6
- trained_up: float32 [4096, 16384], P('fs', 'tp'), may hold values from -0.09375 to 0.09375
- trained_down: float32 [16384, 4096], P('fs', 'tp'), may hold values from -0.046875 to 0.046875
- pre_gain: float32 [4096], P('fs'), may hold values from 0.1 to 1.9
- post_gain: float32 [4096], replicated, may hold values from 0.1 to 1.9
Outputs:
- layer_out: bfloat16 [4, 128, 4096], P('tp', 'fs')
- sampler_up: bfloat16 [4096, 16384], P(None, 'fs')
- sampler_down: bfloat16 [16384, 4096], P('fs')
All inputs are finite; a program needn't handle non-finite values.
Results may differ from a plain program's by a relative error of at most 0.0081.
Values may be sent and summed in bfloat16 or wider, within the bound.
A program may use at most 128 MiB of HBM per device.

v0:
```python
import jax
import jax.numpy as jnp
from jax import lax
from jax.sharding import PartitionSpec as P


def row_norm(values):
    return values * lax.rsqrt(jnp.mean(values * values, axis=-1, keepdims=True) + 1e-06)


def on_device(prompt_tokens, trained_up, trained_down, pre_gain, post_gain):
    folded = (pre_gain[:, None] * trained_up).astype(jnp.bfloat16)
    quarter = lax.all_to_all(folded, "tp", split_axis=0, concat_axis=1, tiled=True)
    owned = lax.all_to_all(quarter, "fs", split_axis=1, concat_axis=0, tiled=True)
    joined = lax.all_gather(owned, "tp", axis=0, tiled=True)
    n_fs = lax.axis_size("fs")
    n_tp = lax.axis_size("tp")
    width = joined.shape[1]
    joined = joined.reshape(n_tp, n_fs, joined.shape[0] // (n_tp * n_fs), width)
    sampler_up = jnp.transpose(joined, (1, 0, 2, 3)).reshape(-1, width)
    sampler_down = lax.all_gather(trained_down.astype(jnp.bfloat16), "tp", axis=1, tiled=True)
    flat = prompt_tokens[0].astype(jnp.float32)
    normed = row_norm(flat).astype(jnp.bfloat16)
    upward = jnp.dot(normed, sampler_up, preferred_element_type=jnp.float32)
    hidden = jnp.square(jax.nn.relu(upward)).astype(jnp.bfloat16)
    summed = lax.psum_scatter(
        jnp.dot(hidden, sampler_down, preferred_element_type=jnp.float32),
        "fs",
        scatter_dimension=0,
        tiled=True,
    )
    layer_out = (row_norm(summed) * post_gain).astype(jnp.bfloat16)
    return (layer_out[None], sampler_up, sampler_down)


def solution(mesh):
    placed = (P("tp", None, None), P("fs", "tp"), P("fs", "tp"), P("fs"), P())
    return jax.shard_map(
        on_device,
        mesh=mesh,
        in_specs=placed,
        out_specs=(P("tp", "fs", None), P(None, "fs"), P("fs", None)),
        check_vma=False,
    )
```

profile of v0, /device:TPU:0, one launch (start us, length us, event | category | flops | bytes accessed | tf_op | source)
XLA Modules:
  0.0 497.2 jit_solution(667741849209752609)
XLA Ops:
  7.2 0.0 all-gather.3.cloned.1.call-start
  7.2 4.6 multiply_convert_fusion
  11.8 52.3 %all_to_all.35 = bf16[4,128,4096]{2,1,0:T(8,128)(2,1)} all-to-all(bf16[4,128,4096]{2,1,0:T(8,128)(2,1)S(1)} %bitcast.25), channel_id=1, replica_groups=mesh['fs'=8,'tp'=4] {'tp'}, dimensions={0} | all-to-all | bytes 8388608 | tf_op jit(solution)/shard_map/all_to_all | solution.py:13
  64.1 6.3 %copy.9 = bf16[128,4,4096]{0,2,1:T(8,128)(2,1)} copy(bf16[128,4,4096]{2,0,1:T(8,128)(2,1)} %bitcast.22) | data formatting | bytes 8388608 | tf_op jit(solution)/shard_map/all_to_all | solution.py:13
  70.4 99.7 %all_to_all.36 = bf16[128,8,2048]{0,2,1:T(8,128)(2,1)} all-to-all(bf16[128,8,2048]{0,2,1:T(8,128)(2,1)} %bitcast.23), channel_id=1, replica_groups=mesh['fs'=8,'tp'=4] {'fs'}, dimensions={1} | all-to-all | bytes 8388608 | tf_op jit(solution)/shard_map/all_to_all | solution.py:14
  170.1 6.4 %copy.10 = bf16[8,128,2048]{2,1,0:T(8,128)(2,1)} copy(bf16[8,128,2048]{1,2,0:T(8,128)(2,1)} %bitcast.24) | data formatting | bytes 8388608 | tf_op jit(solution)/shard_map/all_to_all | solution.py:14
  176.6 0.0 all-gather.3.cloned.1.call-update
  176.6 0.0 copy-start
  176.6 0.0 all-gather.5.cloned.1.call-start
  176.7 6.3 %convert_element_type.28 = bf16[2048,1024]{1,0:T(8,128)(2,1)} convert(f32[2048,1024]{1,0:T(8,128)} %param.7) | non-fusion elementwise | flops 2097152 | bytes 12582912 | tf_op jit(solution)/shard_map/convert_element_type | solution.py:21
  182.9 0.0 all-gather.5.cloned.1.call-update
  182.9 0.0 reduce-scatter.2.cloned.1.call-start
  183.0 0.0 copy-done
  183.0 0.3 fusion.2
  183.3 97.5 %all-gather.3.cloned.1.call-done = bf16[4096,2048]{1,0:T(8,128)(2,1)} async-done(((bf16[1024,2048]{1,0:T(8,128)(2,1)}), bf16[4096,2048]{1,0:T(8,128)(2,1)}) %all-gather.3.cloned.1.call-update) | async-done | bytes 16777232 | tf_op jit(solution)/shard_map/all_gather | solution.py:15
  280.8 14.7 %copy.11 = bf16[8,4,128,2048]{3,2,1,0:T(8,128)(2,1)} copy(bf16[8,4,128,2048]{3,2,0,1:T(8,128)(2,1)} %bitcast.20) | data formatting | bytes 33554432 | tf_op jit(solution)/shard_map/transpose | solution.py:20
  295.5 93.3 %all-gather.5.cloned.1.call-done = bf16[2048,4096]{1,0:T(8,128)(2,1)} async-done(((bf16[2048,1024]{1,0:T(8,128)(2,1)}), bf16[2048,4096]{1,0:T(8,128)(2,1)}) %all-gather.5.cloned.1.call-update) | async-done | bytes 16777232 | tf_op jit(solution)/shard_map/all_gather | solution.py:21
  388.9 0.0 copy-start.1
  388.9 16.4 %fusion.8 = f32[128,4096]{1,0:T(8,128)} fusion(bf16[2048,4096]{1,0:T(8,128)(2,1)} %all-gather.5.cloned.1.call-done, bf16[4096,2048]{1,0:T(8,128)(2,1)} %bitcast.18, bf16[1,128,4096]{2,1,0:T(8,128)(2,1)S(1)} %copy-done, f32[128]{0:T(128)S(1)} %add_rsqrt_fusion.1), kind=kOutput, calls=%fused_computation.10 | convolution fusion | flops 4297326592 | bytes 36700672 | tf_op jit(solution)/shard_map/dot_general | solution.py:27
  405.3 0.0 reduce-scatter.2.cloned.1.call-update
  405.3 68.5 %reduce-scatter.2.cloned.1.call-done = f32[16,4096]{1,0:T(8,128)} async-done(((f32[128,4096]{1,0:T(8,128)}), f32[16,4096]{1,0:T(8,128)}) %reduce-scatter.2.cloned.1.call-update) | async-done | bytes 262160 | tf_op jit(solution)/shard_map/reduce_scatter | solution.py:26
  473.9 1.1 multiply_reduce_fusion
  475.0 0.0 copy-done.1
  475.0 1.7 fusion.11
  476.7 14.1 %copy.13 = bf16[2048,4096]{1,0:T(8,128)(2,1)} copy(bf16[2048,4096]{1,0:T(8,128)(2,1)} %all-gather.5.cloned.1.call-done) | data formatting | bytes 33554432
  (2 shorter events, 0.0 us)
Async XLA Ops:
  7.2 273.6 %all-gather.3.cloned.1.call-start = ((), (), s32[]{:S(2)}) async-start(), calls=%async_computation.3 | async-start | bytes 20971520 | tf_op jit(solution)/shard_map/all_gather | solution.py:15
  176.6 6.4 %copy-start = (bf16[1,128,4096]{2,1,0:T(8,128)(2,1)S(1)}, bf16[1,128,4096]{2,1,0:T(8,128)(2,1)}, u32[]{:S(2)}) copy-start(bf16[1,128,4096]{2,1,0:T(8,128)(2,1)} %param.5) | copy-start | bytes 3145732
  176.6 212.2 %all-gather.5.cloned.1.call-start = ((), (), s32[]{:S(2)}) async-start(), calls=%async_computation.4 | async-start | bytes 20971520 | tf_op jit(solution)/shard_map/all_gather | solution.py:21
  182.9 290.9 %reduce-scatter.2.cloned.1.call-start = ((), (), s32[]{:S(2)}) async-start(), calls=%async_computation.5 | async-start | bytes 2359296 | tf_op jit(solution)/shard_map/reduce_scatter | solution.py:26
  388.9 86.1 %copy-start.1 = (f32[4096]{0:T(1024)S(1)}, f32[4096]{0:T(1024)}, u32[]{:S(2)}) copy-start(f32[4096]{0:T(1024)} %param.9) | copy-start | bytes 49156
Sparse Core Ops, SparseCore 0:
  176.7 104.0 all-gather.2
  282.9 105.8 all-gather.4
  405.4 68.3 reduce-scatter.1
where the time goes:
time: 498 us; the launch traced here: 497 us
  waiting for transfers between devices  259 us (52%)
  blocking collectives  152 us (31%)
  local copies, waits for them, and re-layouts  41.5 us (8%)
  matrix products  16.4 us (3%)
  other arithmetic  14 us (3%)
  between operations  13.8 us (3%)
    all_to_all x1, blocking collectives, on_device(): lax.all_to_all(quarter, 'fs', split_axis=1, concat_axis=0, tiled=True)  99.7 us
    all_gather x1, waiting for transfers between devices, on_device(): joined = lax.all_gather(owned, 'tp', axis=0, tiled=True)  97.5 us
    all_gather x1, waiting for transfers between devices, on_device(): lax.all_gather(trained_down.astype(jnp.bfloat16), 'tp', axis=1, tiled=True)  93.3 us
    reduce_scatter x1, waiting for transfers between devices, on_device(): lax.psum_scatter(jnp.dot(hidden, sampler_down, preferred_element_type=jnp...  68.5 us
    all_to_all x1, blocking collectives, on_device(): lax.all_to_all(folded, 'tp', split_axis=0, concat_axis=1, tiled=True)  52.3 us
    dot_general x1, matrix products, on_device(): jnp.dot(hidden, sampler_down, preferred_element_type=jnp.float32)  16.4 us
    transpose x1, local copies, waits for them, and re-layouts, on_device(): sampler_up = jnp.transpose(joined, (1, 0, 2, 3)).reshape(-1, width)  14.7 us
    unnamed x5, local copies, waits for them, and re-layouts  14.1 us
  transfers between devices with their start and end apart: 3, of which 3 were waited for; matrix products, arithmetic and copies ran while one was open for 4% of the time, Pallas kernels for 0%

commit v1 on v0

--- a/solution.py
+++ b/solution.py
@@ -12,7 +12,10 @@
     folded = (pre_gain[:, None] * trained_up).astype(jnp.bfloat16)
     quarter = lax.all_to_all(folded, "tp", split_axis=0, concat_axis=1, tiled=True)
     owned = lax.all_to_all(quarter, "fs", split_axis=1, concat_axis=0, tiled=True)
-    joined = lax.all_gather(owned, "tp", axis=0, tiled=True)
+    n_dev = lax.axis_size("tp")
+    blocks = jnp.stack([owned for _ in range(n_dev)])
+    blocks = lax.all_to_all(blocks, "tp", split_axis=0, concat_axis=0)
+    joined = jnp.concatenate(blocks, axis=0)
     n_fs = lax.axis_size("fs")
     n_tp = lax.axis_size("tp")
     width = joined.shape[1]

time: 498 us -> 543 us (1.090)
  blocking collectives: 152 us -> 193 us
  waiting for transfers between devices: 259 us -> 249 us
  starting transfers between devices: 0.12 us -> 7.18 us
  local copies, waits for them, and re-layouts: 41.5 us -> 48.4 us
    all_to_all x0 -> x1, waiting for transfers between devices: none -> 183 us  [on_device(): blocks = lax.all_to_all(blocks, 'tp', split_axis=0, concat_axis=0)]
    all_gather x1 -> x0, waiting for transfers between devices: 97.5 us -> none  [on_device(): joined = lax.all_gather(owned, 'tp', axis=0, tiled=True)]
    all_gather x1, waiting for transfers between devices: 93.3 us -> 0.01 us  [on_device(): lax.all_gather(trained_down.astype(jnp.bfloat16), 'tp', axis=1, tiled=True)]
    all_to_all x1, blocking collectives: 52.3 us -> 93.1 us  [on_device(): lax.all_to_all(folded, 'tp', split_axis=0, concat_axis=1, tiled=True)]
    another operation x0 -> x1, local copies, waits for them, and re-layouts: none -> 7.44 us  [on_device(): blocks = jnp.stack([owned for _ in range(n_dev)])]
    all_to_all x0 -> x1, starting transfers between devices: none -> 7.1 us  [on_device(): blocks = lax.all_to_all(blocks, 'tp', split_axis=0, concat_axis=0)]
    unnamed x5 -> x7, local copies, waits for them, and re-layouts: 14.1 us -> 14.1 us
  transfers between devices with their start and end apart: 3 -> 3, of which waited for: 3 -> 2; matrix products, arithmetic and copies ran while one was open for 4% -> 7% of each run, Pallas kernels for 0% -> 0%
where the time goes in v1:
time: 543 us; the launch traced here: 542 us
  waiting for transfers between devices  249 us (46%)
  blocking collectives  193 us (36%)
  local copies, waits for them, and re-layouts  48.4 us (9%)
  matrix products  16.4 us (3%)
  between operations  14.1 us (3%)
  other arithmetic  13.8 us (3%)
  starting transfers between devices  7.18 us (1%)
    all_to_all x1, waiting for transfers between devices, on_device(): blocks = lax.all_to_all(blocks, 'tp', split_axis=0, concat_axis=0)  183 us
    all_to_all x1, blocking collectives, on_device(): lax.all_to_all(quarter, 'fs', split_axis=1, concat_axis=0, tiled=True)  100 us
    all_to_all x1, blocking collectives, on_device(): lax.all_to_all(folded, 'tp', split_axis=0, concat_axis=1, tiled=True)  93.1 us
    reduce_scatter x1, waiting for transfers between devices, on_device(): lax.psum_scatter(jnp.dot(hidden, sampler_down, preferred_element_type=jnp...  66.3 us
    dot_general x1, matrix products, on_device(): jnp.dot(hidden, sampler_down, preferred_element_type=jnp.float32)  16.4 us
    transpose x1, local copies, waits for them, and re-layouts, on_device(): sampler_up = jnp.transpose(joined, (1, 0, 2, 3)).reshape(-1, width)  14.2 us
    unnamed x7, local copies, waits for them, and re-layouts  14.1 us
  transfers between devices with their start and end apart: 3, of which 2 were waited for; matrix products, arithmetic and copies ran while one was open for 7% of the time, Pallas kernels for 0%

profile of v1, /device:TPU:0, one launch (start us, length us, event | category | flops | bytes accessed | tf_op | source)
XLA Modules:
  0.0 542.1 jit_solution(11014088258566491424)
XLA Ops:
  7.2 0.0 copy-start.2
  7.2 0.0 all-gather.2.cloned.1.call-start
  7.2 6.1 %convert_element_type.28 = bf16[2048,1024]{1,0:T(8,128)(2,1)} convert(f32[2048,1024]{1,0:T(8,128)} %param.7) | non-fusion elementwise | flops 2097152 | bytes 12582912 | tf_op jit(solution)/shard_map/convert_element_type | solution.py:24
  13.3 0.0 all-gather.2.cloned.1.call-update
  13.3 0.0 copy-done.2
  13.4 4.6 multiply_convert_fusion
  17.9 93.1 %all_to_all.37 = bf16[4,128,4096]{2,1,0:T(8,128)(2,1)} all-to-all(bf16[4,128,4096]{2,1,0:T(8,128)(2,1)S(1)} %bitcast.24), channel_id=1, replica_groups=mesh['fs'=8,'tp'=4] {'tp'}, dimensions={0} | all-to-all | bytes 8388608 | tf_op jit(solution)/shard_map/all_to_all | solution.py:13
  111.0 6.3 %copy.9 = bf16[128,4,4096]{0,2,1:T(8,128)(2,1)} copy(bf16[128,4,4096]{2,0,1:T(8,128)(2,1)} %bitcast.21) | data formatting | bytes 8388608 | tf_op jit(solution)/shard_map/all_to_all | solution.py:13
  117.4 100.1 %all_to_all.38 = bf16[128,8,2048]{0,2,1:T(8,128)(2,1)} all-to-all(bf16[128,8,2048]{0,2,1:T(8,128)(2,1)} %bitcast.22), channel_id=1, replica_groups=mesh['fs'=8,'tp'=4] {'fs'}, dimensions={1} | all-to-all | bytes 8388608 | tf_op jit(solution)/shard_map/all_to_all | solution.py:14
  217.5 6.4 %copy.10 = bf16[8,128,2048]{2,1,0:T(8,128)(2,1)} copy(bf16[8,128,2048]{1,2,0:T(8,128)(2,1)} %bitcast.23) | data formatting | bytes 8388608 | tf_op jit(solution)/shard_map/all_to_all | solution.py:14
  223.9 7.4 %stack.10 = bf16[4,1024,2048]{2,1,0:T(8,128)(2,1)} broadcast(bf16[1024,2048]{1,0:T(8,128)(2,1)} %bitcast.20), dimensions={1,2} | broadcast | bytes 20971520 | tf_op jit(solution)/shard_map/stack | solution.py:16
  231.3 0.0 copy-start
  231.3 7.1 %all-to-all-start.2 = ((bf16[4,1024,2048]{2,1,0:T(8,128)(2,1)}), bf16[4,1024,2048]{2,1,0:T(8,128)(2,1)}, u32[]{:S(2)}, u32[]{:S(2)}) async-start(bf16[4,1024,2048]{2,1,0:T(8,128)(2,1)} %stack.10), calls=%async_computation.2 | async-start | bytes 33554432 | tf_op jit(solution)/shard_map/all_to_all | solution.py:17
  238.5 0.0 reduce-scatter.2.cloned.1.call-start
  238.5 0.0 copy-done
  238.5 0.3 fusion.2
  238.8 182.7 %all-to-all-done.2 = bf16[4,1024,2048]{2,1,0:T(8,128)(2,1)} async-done(((bf16[4,1024,2048]{2,1,0:T(8,128)(2,1)}), bf16[4,1024,2048]{2,1,0:T(8,128)(2,1)}, u32[]{:S(2)}, u32[]{:S(2)}) %all-to-all-start.2) | async-done | bytes 16777248 | tf_op jit(solution)/shard_map/all_to_all | solution.py:17
  421.5 14.2 %copy.11 = bf16[8,4,128,2048]{3,2,1,0:T(8,128)(2,1)} copy(bf16[8,4,128,2048]{3,2,0,1:T(8,128)(2,1)} %bitcast.7) | data formatting | bytes 33554432 | tf_op jit(solution)/shard_map/transpose | solution.py:23
  435.6 0.0 all-gather.2.cloned.1.call-done
  435.6 0.0 copy-start.1
  435.6 16.4 %fusion.8 = f32[128,4096]{1,0:T(8,128)} fusion(bf16[2048,4096]{1,0:T(8,128)(2,1)} %all-gather.2.cloned.1.call-done, bf16[4096,2048]{1,0:T(8,128)(2,1)} %bitcast.18, bf16[1,128,4096]{2,1,0:T(8,128)(2,1)S(1)} %copy-done, f32[128]{0:T(128)S(1)} %add_rsqrt_fusion.1), kind=kOutput, calls=%fused_computation.10 | convolution fusion | flops 4297326592 | bytes 36700672 | tf_op jit(solution)/shard_map/dot_general | solution.py:30
  452.1 0.0 reduce-scatter.2.cloned.1.call-update
  452.1 66.3 %reduce-scatter.2.cloned.1.call-done = f32[16,4096]{1,0:T(8,128)} async-done(((f32[128,4096]{1,0:T(8,128)}), f32[16,4096]{1,0:T(8,128)}) %reduce-scatter.2.cloned.1.call-update) | async-done | bytes 262160 | tf_op jit(solution)/shard_map/reduce_scatter | solution.py:29
  518.4 1.1 multiply_reduce_fusion
  519.5 0.0 copy-done.1
  519.5 1.7 fusion.11
  521.2 14.1 %copy.13 = bf16[2048,4096]{1,0:T(8,128)(2,1)} copy(bf16[2048,4096]{1,0:T(8,128)(2,1)} %all-gather.2.cloned.1.call-done) | data formatting | bytes 33554432
  (2 shorter events, 0.0 us)
Async XLA Ops:
  7.2 6.2 %copy-start.2 = (f32[512]{0:T(512)S(1)}, f32[512]{0:T(512)}, u32[]{:S(2)}) copy-start(f32[512]{0:T(512)} %param.8) | copy-start | bytes 6148
  7.2 428.5 %all-gather.2.cloned.1.call-start = ((), (), s32[]{:S(2)}) async-start(), calls=%async_computation.4 | async-start | bytes 20971520 | tf_op jit(solution)/shard_map/all_gather | solution.py:24
  231.3 7.2 %copy-start = (bf16[1,128,4096]{2,1,0:T(8,128)(2,1)S(1)}, bf16[1,128,4096]{2,1,0:T(8,128)(2,1)}, u32[]{:S(2)}) copy-start(bf16[1,128,4096]{2,1,0:T(8,128)(2,1)} %param.5) | copy-start | bytes 3145732
  231.3 190.1 %all-to-all-start.2 = ((bf16[4,1024,2048]{2,1,0:T(8,128)(2,1)}), bf16[4,1024,2048]{2,1,0:T(8,128)(2,1)}, u32[]{:S(2)}, u32[]{:S(2)}) async-start(bf16[4,1024,2048]{2,1,0:T(8,128)(2,1)} %stack.10), calls=%async_computation.2 | async-start | bytes 33554432 | tf_op jit(solution)/shard_map/all_to_all | solution.py:17
  238.5 279.9 %reduce-scatter.2.cloned.1.call-start = ((), (), s32[]{:S(2)}) async-start(), calls=%async_computation.5 | async-start | bytes 2359296 | tf_op jit(solution)/shard_map/reduce_scatter | solution.py:29
  435.6 83.9 %copy-start.1 = (f32[4096]{0:T(1024)S(1)}, f32[4096]{0:T(1024)}, u32[]{:S(2)}) copy-start(f32[4096]{0:T(1024)} %param.9) | copy-start | bytes 49156
Sparse Core Ops, SparseCore 0:
  13.5 148.6 all-gather.1
  452.2 66.1 reduce-scatter.1

commit v2 on v0

--- a/solution.py
+++ b/solution.py
@@ -18,7 +18,9 @@
     width = joined.shape[1]
     joined = joined.reshape(n_tp, n_fs, joined.shape[0] // (n_tp * n_fs), width)
     sampler_up = jnp.transpose(joined, (1, 0, 2, 3)).reshape(-1, width)
-    sampler_down = lax.all_gather(trained_down.astype(jnp.bfloat16), "tp", axis=1, tiled=True)
+    block = trained_down.astype(jnp.bfloat16)
+    pieces = lax.all_gather(block, "tp")
+    sampler_down = jnp.concatenate(pieces, axis=1)
     flat = prompt_tokens[0].astype(jnp.float32)
     normed = row_norm(flat).astype(jnp.bfloat16)
     upward = jnp.dot(normed, sampler_up, preferred_element_type=jnp.float32)

time: 498 us -> 437 us (0.88)
  waiting for transfers between devices: 259 us -> 143 us
  blocking collectives: 152 us -> 193 us
  local copies, waits for them, and re-layouts: 41.5 us -> 56.5 us
    all_gather x1, waiting for transfers between devices: 93.3 us -> 0.02 us  [on_device(): pieces = lax.all_gather(block, 'tp')]
    all_to_all x1, blocking collectives: 52.3 us -> 93.2 us  [on_device(): lax.all_to_all(folded, 'tp', split_axis=0, concat_axis=1, tiled=True)]
    all_gather x1, waiting for transfers between devices: 97.5 us -> 74.1 us  [on_device(): joined = lax.all_gather(owned, 'tp', axis=0, tiled=True)]
    all_gather x0 -> x1, local copies, waits for them, and re-layouts: none -> 19.1 us  [on_device(): pieces = lax.all_gather(block, 'tp')]
    unnamed x5 -> x7, local copies, waits for them, and re-layouts: 14.1 us -> 10.3 us
  transfers between devices with their start and end apart: 3 -> 3, of which waited for: 3 -> 2; matrix products, arithmetic and copies ran while one was open for 4% -> 11% of each run, Pallas kernels for 0% -> 0%
where the time goes in v2:
time: 437 us
  blocking collectives  193 us (44%)
  waiting for transfers between devices  143 us (33%)
  local copies, waits for them, and re-layouts  56.5 us (13%)
  matrix products  16.4 us (4%)
  between operations  13.8 us (3%)
  other arithmetic  13.7 us (3%)
    all_to_all x1, blocking collectives, on_device(): lax.all_to_all(quarter, 'fs', split_axis=1, concat_axis=0, tiled=True)  100 us
    all_to_all x1, blocking collectives, on_device(): lax.all_to_all(folded, 'tp', split_axis=0, concat_axis=1, tiled=True)  93.2 us
    all_gather x1, waiting for transfers between devices, on_device(): joined = lax.all_gather(owned, 'tp', axis=0, tiled=True)  74.1 us
    reduce_scatter x1, waiting for transfers between devices, on_device(): lax.psum_scatter(jnp.dot(hidden, sampler_down, preferred_element_type=jnp...  68.7 us
    all_gather x1, local copies, waits for them, and re-layouts, on_device(): pieces = lax.all_gather(block, 'tp')  19.1 us
    dot_general x1, matrix products, on_device(): jnp.dot(hidden, sampler_down, preferred_element_type=jnp.float32)  16.4 us
    transpose x1, local copies, waits for them, and re-layouts, on_device(): sampler_up = jnp.transpose(joined, (1, 0, 2, 3)).reshape(-1, width)  14.2 us
    unnamed x7, local copies, waits for them, and re-layouts  10.3 us
  transfers between devices with their start and end apart: 3, of which 2 were waited for; matrix products, arithmetic and copies ran while one was open for 11% of the time, Pallas kernels for 0%

profile of v2, /device:TPU:0, one launch (start us, length us, event | category | flops | bytes accessed | tf_op | source)
XLA Modules:
  0.0 436.8 jit_solution(10299181796042101305)
XLA Ops:
  7.2 0.0 copy-start.2
  7.2 0.0 all-gather.6.cloned.1.call-start
  7.2 6.1 %convert_element_type.28 = bf16[2048,1024]{1,0:T(8,128)(2,1)} convert(f32[2048,1024]{1,0:T(8,128)} %param.7) | non-fusion elementwise | flops 2097152 | bytes 12582912 | tf_op jit(solution)/shard_map/convert_element_type | solution.py:21
  13.3 0.0 all-gather.6.cloned.1.call-update
  13.3 0.0 all-gather.4.cloned.1.call-start
  13.4 0.0 copy-done.2
  13.4 4.6 %multiply_convert_fusion = bf16[512,4096]{1,0:T(8,128)(2,1)S(1)} fusion(f32[512,4096]{1,0:T(8,128)} %param.6, f32[512]{0:T(512)S(1)} %copy-done.2), kind=kLoop, calls=%fused_computation | loop fusion | flops 4194304 | bytes 12584960 | tf_op jit(solution)/shard_map/convert_element_type | solution.py:12
  18.0 93.2 %all_to_all.35 = bf16[4,128,4096]{2,1,0:T(8,128)(2,1)} all-to-all(bf16[4,128,4096]{2,1,0:T(8,128)(2,1)S(1)} %bitcast.33), channel_id=1, replica_groups=mesh['fs'=8,'tp'=4] {'tp'}, dimensions={0} | all-to-all | bytes 8388608 | tf_op jit(solution)/shard_map/all_to_all | solution.py:13
  111.1 6.3 %copy.11 = bf16[128,4,4096]{0,2,1:T(8,128)(2,1)} copy(bf16[128,4,4096]{2,0,1:T(8,128)(2,1)} %bitcast.30) | data formatting | bytes 8388608 | tf_op jit(solution)/shard_map/all_to_all | solution.py:13
  117.4 100.1 %all_to_all.36 = bf16[128,8,2048]{0,2,1:T(8,128)(2,1)} all-to-all(bf16[128,8,2048]{0,2,1:T(8,128)(2,1)} %bitcast.31), channel_id=1, replica_groups=mesh['fs'=8,'tp'=4] {'fs'}, dimensions={1} | all-to-all | bytes 8388608 | tf_op jit(solution)/shard_map/all_to_all | solution.py:14
  217.5 0.0 copy-start
  217.5 6.6 %copy.12 = bf16[8,128,2048]{2,1,0:T(8,128)(2,1)} copy(bf16[8,128,2048]{1,2,0:T(8,128)(2,1)} %bitcast.32) | data formatting | bytes 8388608 | tf_op jit(solution)/shard_map/all_to_all | solution.py:14
  224.2 0.0 all-gather.4.cloned.1.call-update
  224.2 0.0 reduce-scatter.2.cloned.1.call-start
  224.2 0.0 copy-done
  224.2 0.3 fusion.2
  224.5 0.0 all-gather.6.cloned.1.call-done
  224.6 19.1 %copy.14 = bf16[4,2048,1024]{2,0,1:T(4,128)(2,1)S(1)} copy(bf16[4,2048,1024]{2,1,0:T(8,128)(2,1)} %bitcast.27) | data formatting | bytes 33554432 | tf_op jit(solution)/shard_map/all_gather | solution.py:22
  243.7 10.3 %copy.15 = bf16[256,8,4,1024]{3,1,2,0:T(8,128)(2,1)} copy(bf16[256,8,4,1024]{3,2,1,0:T(4,128)(2,1)S(1)} %bitcast.26) | data formatting | bytes 33554432
  253.9 74.1 %all-gather.4.cloned.1.call-done = bf16[4096,2048]{1,0:T(8,128)(2,1)} async-done(((bf16[1024,2048]{1,0:T(8,128)(2,1)}), bf16[4096,2048]{1,0:T(8,128)(2,1)}) %all-gather.4.cloned.1.call-update) | async-done | bytes 16777232 | tf_op jit(solution)/shard_map/all_gather | solution.py:15
  328.1 14.2 %copy.13 = bf16[8,4,128,2048]{3,2,1,0:T(8,128)(2,1)} copy(bf16[8,4,128,2048]{3,2,0,1:T(8,128)(2,1)} %bitcast.28) | data formatting | bytes 33554432 | tf_op jit(solution)/shard_map/transpose | solution.py:20
  342.3 0.0 copy-start.1
  342.3 16.4 %fusion.8 = f32[128,4096]{1,0:T(8,128)} fusion(bf16[2048,4096]{1,0:T(8,128)(2,1)} %bitcast.22, bf16[4096,2048]{1,0:T(8,128)(2,1)} %bitcast.24, bf16[1,128,4096]{2,1,0:T(8,128)(2,1)S(1)} %copy-done, f32[128]{0:T(128)S(1)} %add_rsqrt_fusion.1), kind=kOutput, calls=%fused_computation.10 | convolution fusion | flops 4297326592 | bytes 36700672 | tf_op jit(solution)/shard_map/dot_general | solution.py:29
  358.7 0.0 reduce-scatter.2.cloned.1.call-update
  358.7 68.7 %reduce-scatter.2.cloned.1.call-done = f32[16,4096]{1,0:T(8,128)} async-done(((f32[128,4096]{1,0:T(8,128)}), f32[16,4096]{1,0:T(8,128)}) %reduce-scatter.2.cloned.1.call-update) | async-done | bytes 262160 | tf_op jit(solution)/shard_map/reduce_scatter | solution.py:28
  427.5 1.1 multiply_reduce_fusion
  428.6 0.0 copy-done.1
  428.6 1.7 fusion.11
  (2 shorter events, 0.0 us)
Async XLA Ops:
  7.2 6.2 %copy-start.2 = (f32[512]{0:T(512)S(1)}, f32[512]{0:T(512)}, u32[]{:S(2)}) copy-start(f32[512]{0:T(512)} %param.8) | copy-start | bytes 6148
  7.2 217.4 %all-gather.6.cloned.1.call-start = ((), (), s32[]{:S(2)}) async-start(), calls=%async_computation.5 | async-start | bytes 20971520 | tf_op jit(solution)/shard_map/all_gather | solution.py:22
  13.3 314.8 %all-gather.4.cloned.1.call-start = ((), (), s32[]{:S(2)}) async-start(), calls=%async_computation.3 | async-start | bytes 20971520 | tf_op jit(solution)/shard_map/all_gather | solution.py:15
  217.5 6.7 %copy-start = (bf16[1,128,4096]{2,1,0:T(8,128)(2,1)S(1)}, bf16[1,128,4096]{2,1,0:T(8,128)(2,1)}, u32[]{:S(2)}) copy-start(bf16[1,128,4096]{2,1,0:T(8,128)(2,1)} %param.5) | copy-start | bytes 3145732
  224.2 203.3 %reduce-scatter.2.cloned.1.call-start = ((), (), s32[]{:S(2)}) async-start(), calls=%async_computation.4 | async-start | bytes 2359296 | tf_op jit(solution)/shard_map/reduce_scatter | solution.py:28
  342.3 86.3 %copy-start.1 = (f32[4096]{0:T(1024)S(1)}, f32[4096]{0:T(1024)}, u32[]{:S(2)}) copy-start(f32[4096]{0:T(1024)} %param.9) | copy-start | bytes 49156
Sparse Core Ops, SparseCore 0:
  13.4 148.6 all-gather.5
  224.3 103.7 all-gather.3
  358.8 68.5 reduce-scatter.1
